TPU v7x, 512 devices: a 4x2x32 block of a 4x8x32 slice. The times are simulated.
512 devices in a mesh: grp: 2 (over y), sp: 64 (over z, core), tp: 4 (over x).
Axes of the slice: x: 4, y: 2, z: 32, core: 2. Of those that a mesh axis runs over, the one named last changes fastest.
The devices are a block of a 4x8x32 slice.
Arguments:
- tokens: bfloat16 [65536, 2048], P(('grp', 'sp')), parts along dimension 0, may hold values from -6 to 6
- gate_in: bfloat16 [2, 2048, 512], P(None, 'sp', 'tp'), may hold values from -0.125 to 0.125
- gate_conv: bfloat16 [2, 2048, 512], P(None, 'sp', 'tp'), may hold values from -0.125 to 0.125
- value_in: bfloat16 [2, 2048, 512], P(None, 'sp', 'tp'), may hold values from -0.125 to 0.125
- out_weight: bfloat16 [2, 512, 2048], P(None, None, 'sp'), may hold values from -0.25 to 0.25
- conv_taps: float32 [2, 3, 512], replicated, may hold values from -7 to 7
- pre_gain: float32 [2, 2048], replicated, may hold values from 0.1 to 1.9
- mix_gain: float32 [2, 512], replicated, may hold values from 0.1 to 1.9
- post_gain: float32 [2, 2048], replicated, may hold values from 0.1 to 1.9
Outputs:
- result: bfloat16 [65536, 2048], P(('grp', 'sp', 'tp')), parts along dimension 0
There are 2 independent parts, one for each index of `grp`. A program takes and returns all parts, laid end to end along the dimension named above; an argument that names none is the same for every part. Nothing has to cross between parts.
All inputs are finite; a program needn't handle non-finite values.
Results may differ from a plain program's by a relative error of at most 0.011.
Values may be sent and summed in bfloat16 or wider, within the bound.
A program may use at most 64 MiB of HBM per device.

v0:
```python
import jax
import jax.numpy as jnp
from jax import lax
from jax.sharding import PartitionSpec as P

EPS = 1e-06


def rows_first(arrays, axis, dims):
    turned = [jnp.moveaxis(a, dim, 0) for a, dim in zip(arrays, dims)]
    widths = [t[0].size for t in turned]
    both = jnp.concatenate([t.reshape(-1, w) for t, w in zip(turned, widths)], axis=1)
    whole = lax.all_gather(both, axis, axis=0, tiled=True)
    tiles = jnp.split(whole, [sum(widths[:k]) for k in range(1, len(widths))], axis=1)
    return tuple(
        (
            jnp.moveaxis(b.reshape(-1, *t.shape[1:]), 0, dim)
            for b, t, dim in zip(tiles, turned, dims)
        )
    )


def passed_along(x, axis, by):
    length = lax.axis_size(axis)
    pairs = [(i, i + by) for i in range(length) if 0 <= i + by < length]
    return lax.ppermute(x, axis, pairs)


def in_order(tiles, dim):
    shape = list(tiles.shape[1:])
    shape[dim] *= tiles.shape[0]
    return jnp.moveaxis(tiles, 0, dim).reshape(shape)


def copy_for_each(x, axis):
    length = lax.axis_size(axis)
    return lax.all_to_all(jnp.broadcast_to(x[None], (length, *x.shape)), axis, 0, 0, tiled=True)


def gather_directly(x, axis, dim):
    return in_order(copy_for_each(x, axis), dim)


def rms_norm(values, gain):
    return values * lax.rsqrt(jnp.mean(values * values, axis=-1, keepdims=True) + EPS) * gain


def stored(values):
    return lax.optimization_barrier(values.astype(jnp.bfloat16))


def per_device(
    tokens, gate_in, gate_conv, value_in, out_weight, conv_taps, pre_gain, mix_gain, post_gain
):
    layer_count = gate_in.shape[0]
    channel_count = gate_in.shape[2]
    tap_count = conv_taps.shape[1]
    row_count = tokens.shape[0]
    tp_size = lax.axis_size("tp")
    tp_index = lax.axis_index("tp")
    row_share = row_count // tp_size
    all_outer, all_inner, all_values, all_out = rows_first(
        (gate_in, gate_conv, value_in, out_weight), "sp", (1, 1, 1, 2)
    )
    stream = tokens.astype(jnp.float32)
    for layer_index in range(layer_count):
        is_last = layer_index == layer_count - 1
        normed = stored(rms_norm(stream, pre_gain[layer_index]))
        outer_whole = all_outer[layer_index]
        inner_whole = all_inner[layer_index]
        value_whole = all_values[layer_index]
        out_whole = all_out[layer_index]
        outer = stored(jnp.dot(normed, outer_whole, preferred_element_type=jnp.float32))
        inner = stored(jnp.dot(normed, inner_whole, preferred_element_type=jnp.float32))
        values = stored(jnp.dot(normed, value_whole, preferred_element_type=jnp.float32))
        gated = stored(inner.astype(jnp.float32) * values.astype(jnp.float32))
        before = passed_along(gated[row_count - (tap_count - 1) :], "sp", 1)
        padded = jnp.concatenate([before, gated], axis=0)
        taps_here = lax.dynamic_slice_in_dim(
            conv_taps[layer_index], tp_index * channel_count, channel_count, 1
        )
        filtered = jnp.zeros((row_count, channel_count), jnp.float32)
        for tap_index in range(tap_count):
            filtered = filtered + taps_here[tap_index] * padded[
                tap_index : tap_index + row_count
            ].astype(jnp.float32)
        mixed_raw = stored(outer.astype(jnp.float32) * filtered)
        if is_last:
            arrived = lax.all_to_all(mixed_raw, "tp", split_axis=0, concat_axis=1, tiled=True)
            residual = lax.dynamic_slice_in_dim(stream, tp_index * row_share, row_share, 0)
        else:
            arrived = gather_directly(mixed_raw, "tp", 1)
            residual = stream
        mixed = stored(rms_norm(arrived.astype(jnp.float32), mix_gain[layer_index]))
        branch = stored(jnp.dot(mixed, out_whole, preferred_element_type=jnp.float32))
        stream = residual + rms_norm(branch.astype(jnp.float32), post_gain[layer_index])
    return stream.astype(jnp.bfloat16)


def solution(mesh):
    placed = (
        P(("grp", "sp"), None),
        P(None, "sp", "tp"),
        P(None, "sp", "tp"),
        P(None, "sp", "tp"),
        P(None, None, "sp"),
        P(),
        P(),
        P(),
        P(),
    )
    return jax.shard_map(
        per_device,
        mesh=mesh,
        in_specs=placed,
        out_specs=P(("grp", "sp", "tp"), None),
        check_vma=False,
    )
```

profile of v0, /device:TPU:33, one launch (start us, length us, event | category | flops | bytes accessed | tf_op | source)
XLA Modules:
  0.0 236.6 jit_solution(8318668567519101586)
XLA Ops:
  6.6 1.0 copy.27
  7.6 0.7 copy_bitcast_fusion.2
  8.3 0.7 copy_bitcast_fusion
  9.0 0.7 pad_maximum_fusion.2
  9.7 2.1 fusion.2
  11.9 1.9 fusion.4
  13.9 162.1 %all-gather.2.cloned.1.call-done = bf16[2048,1792]{1,0:T(8,128)(2,1)} async-done(((bf16[32,1792]{1,0:T(8,128)(2,1)}), bf16[2048,1792]{1,0:T(8,128)(2,1)}) %all-gather.2.cloned.1.call-update) | async-done | bytes 7340048 | tf_op jit(solution)/shard_map/all_gather | solution.py:13
  176.0 2.4 %slice_bitcast_fusion.6 = (bf16[256,2,8,128]{3,2,1,0:T(8,128)(2,1)S(1)}, bf16[256,2,8,128]{3,2,1,0:T(8,128)(2,1)S(1)}, bf16[256,2,8,128]{3,2,1,0:T(8,128)(2,1)S(1)}) fusion(bf16[2048,1792]{1,0:T(8,128)(2,1)} %all-gather.2.cloned.1.call-done), kind=kLoop, calls=%fused_computation.33 | loop fusion | bytes 6291456
  178.5 1.9 copy-done.3
  180.4 0.7 convolution_convert_fusion.6
  181.2 0.7 convolution_convert_fusion.5
  181.9 2.6 %collective-permute-start = (bf16[2,128]{1,0:T(2,128)(2,1)S(1)}, bf16[2,128]{1,0:T(2,128)(2,1)S(1)}, u32[]{:S(2)}, u32[]{:S(2)}) collective-permute-start(bf16[2,128]{1,0:T(2,128)(2,1)S(1)} %slice.121), channel_id=1, source_target_pairs={{0,4},{4,8},{8,12},{12,16},{16,20},{20,24},{24,28},{28,32},{32,36}... | collective-permute-start | bytes 1544 | tf_op jit(solution)/shard_map/ppermute | solution.py:26
  184.7 0.7 convolution_convert_fusion.7
  185.4 0.2 copy-done.8
  185.9 0.8 broadcast_in_dim.2
  186.7 3.9 %all-to-all-start = ((bf16[4,512,128]{1,2,0:T(8,128)(2,1)}), bf16[4,512,128]{1,2,0:T(8,128)(2,1)S(1)}, u32[]{:S(2)}, u32[]{:S(2)}) async-start(bf16[4,512,128]{1,2,0:T(8,128)(2,1)} %broadcast_in_dim.2), calls=%async_computation | async-start | bytes 1048576 | tf_op jit(solution)/shard_map/all_to_all | solution.py:37
  190.6 4.7 %split.19 = bf16[2048,1024]{1,0:T(8,128)(2,1)} slice(bf16[2048,1792]{1,0:T(8,128)(2,1)} %all-gather.2.cloned.1.call-done), slice={[0:2048], [768:1792]} | slice | bytes 8388608 | tf_op jit(solution)/shard_map/split | solution.py:14
  195.3 6.5 %copy.20 = bf16[2048,1024]{0,1:T(8,128)(2,1)} copy(bf16[2048,1024]{1,0:T(8,128)(2,1)} %split.19) | data formatting | bytes 8388608 | tf_op jit(solution)/shard_map/reshape | solution.py:17
  202.2 2.9 %convolution_convert_fusion = bf16[512,2048]{1,0:T(8,128)(2,1)S(1)} fusion(bf16[512,512]{0,1:T(8,128)(2,1)S(1)} %fusion.10, bf16[2,512,2048]{2,1,0:T(8,128)(2,1)} %bitcast.115), kind=kOutput, calls=%fused_computation.12 | convolution fusion | flops 1074790400 | bytes 4718592 | tf_op jit(solution)/shard_map/dot_general | solution.py:95
  205.1 0.5 fusion
  205.5 1.1 multiply_reduce_fusion
  206.7 0.4 multiply_convert_fusion
  207.1 1.5 copy-done.1
  208.7 0.7 convolution_convert_fusion.3
  209.4 0.5 copy-done.7
  209.9 0.7 convolution_convert_fusion.2
  210.7 4.1 %collective-permute-start.1 = (bf16[2,128]{1,0:T(2,128)(2,1)S(1)}, bf16[2,128]{1,0:T(2,128)(2,1)S(1)}, u32[]{:S(2)}, u32[]{:S(2)}) collective-permute-start(bf16[2,128]{1,0:T(2,128)(2,1)S(1)} %slice.128), channel_id=1, source_target_pairs={{0,4},{4,8},{8,12},{12,16},{16,20},{20,24},{24,28},{28,32},{32,36}... | collective-permute-start | bytes 1544 | tf_op jit(solution)/shard_map/ppermute | solution.py:26
  214.8 0.7 convolution_convert_fusion.4
  215.8 9.2 %all_to_all.18 = bf16[4,128,128]{1,2,0:T(8,128)(2,1)S(1)} all-to-all(bf16[4,128,128]{1,2,0:T(8,128)(2,1)S(1)} %copy.19), channel_id=1, replica_groups=mesh['grp'=2,'sp'=64,'tp'=4] {'tp'}, dimensions={0} | all-to-all | bytes 262144 | tf_op jit(solution)/shard_map/all_to_all | solution.py:89
  225.2 2.1 convolution_convert_fusion.1
  227.3 0.2 fusion.5
  227.5 2.3 fusion.8
  (56 shorter events, 1.6 us)
Async XLA Ops:
  6.5 1.7 copy-start
  6.6 5.3 %copy-start.2 = (bf16[512,2048]{1,0:T(8,128)(2,1)S(1)}, bf16[512,2048]{1,0:T(8,128)(2,1)}, u32[]{:S(2)}) copy-start(bf16[512,2048]{1,0:T(8,128)(2,1)} %param.9) | copy-start | bytes 6291460
  6.6 5.3 %copy-start.10 = (f32[2,2048]{1,0:T(2,128)S(1)}, f32[2,2048]{1,0:T(2,128)}, u32[]{:S(2)}) copy-start(f32[2,2048]{1,0:T(2,128)} %param.15) | copy-start | bytes 49156
  6.6 169.4 %all-gather.2.cloned.1.call-start = ((), (), s32[]{:S(2)}) async-start(), calls=%async_computation.2 | async-start | bytes 7454720 | tf_op jit(solution)/shard_map/all_gather | solution.py:13
  11.9 2.0 copy-start.12
  11.9 2.0 copy-start.13
  178.4 2.0 copy-start.3
  178.5 2.7 %copy-start.4 = (bf16[256,2,8,128]{3,2,0,1:T(8,128)(2,1)}, bf16[256,2,8,128]{3,2,0,1:T(8,128)(2,1)S(1)}, u32[]{:S(2)}) copy-start(bf16[256,2,8,128]{3,2,0,1:T(8,128)(2,1)S(1)} %copy.35) | copy-start | bytes 3145732
  181.2 3.5 %copy-start.6 = (bf16[256,2,8,128]{3,2,0,1:T(8,128)(2,1)}, bf16[256,2,8,128]{3,2,0,1:T(8,128)(2,1)S(1)}, u32[]{:S(2)}) copy-start(bf16[256,2,8,128]{3,2,0,1:T(8,128)(2,1)S(1)} %copy.34) | copy-start | bytes 3145732
  181.9 3.7 %collective-permute-start = (bf16[2,128]{1,0:T(2,128)(2,1)S(1)}, bf16[2,128]{1,0:T(2,128)(2,1)S(1)}, u32[]{:S(2)}, u32[]{:S(2)}) collective-permute-start(bf16[2,128]{1,0:T(2,128)(2,1)S(1)} %slice.121), channel_id=1, source_target_pairs={{0,4},{4,8},{8,12},{12,16},{16,20},{20,24},{24,28},{28,32},{32,36}... | collective-permute-start | bytes 1544 | tf_op jit(solution)/shard_map/ppermute | solution.py:26
  184.7 1.0 copy-start.8
  184.7 5.9 %copy-start.11 = (f32[2,2048]{1,0:T(2,128)S(1)}, f32[2,2048]{1,0:T(2,128)}, u32[]{:S(2)}) copy-start(f32[2,2048]{1,0:T(2,128)} %param.17) | copy-start | bytes 49156
  186.7 15.1 %all-to-all-start = ((bf16[4,512,128]{1,2,0:T(8,128)(2,1)}), bf16[4,512,128]{1,2,0:T(8,128)(2,1)S(1)}, u32[]{:S(2)}, u32[]{:S(2)}) async-start(bf16[4,512,128]{1,2,0:T(8,128)(2,1)} %broadcast_in_dim.2), calls=%async_computation | async-start | bytes 1048576 | tf_op jit(solution)/shard_map/all_to_all | solution.py:37
  206.7 2.0 copy-start.1
  206.7 2.0 copy-start.5
  208.7 1.2 copy-start.7
  209.9 4.9 %copy-start.9 = (bf16[256,2,8,128]{3,2,0,1:T(8,128)(2,1)S(1)}, bf16[256,2,8,128]{3,2,0,1:T(8,128)(2,1)}, u32[]{:S(2)}) copy-start(bf16[256,2,8,128]{3,2,0,1:T(8,128)(2,1)} %copy-done.8) | copy-start | bytes 3145732
  210.7 4.9 %collective-permute-start.1 = (bf16[2,128]{1,0:T(2,128)(2,1)S(1)}, bf16[2,128]{1,0:T(2,128)(2,1)S(1)}, u32[]{:S(2)}, u32[]{:S(2)}) collective-permute-start(bf16[2,128]{1,0:T(2,128)(2,1)S(1)} %slice.128), channel_id=1, source_target_pairs={{0,4},{4,8},{8,12},{12,16},{16,20},{20,24},{24,28},{28,32},{32,36}... | collective-permute-start | bytes 1544 | tf_op jit(solution)/shard_map/ppermute | solution.py:26
Sparse Core Ops, SparseCore 0:
  9.8 166.0 all-gather.1
where the time goes:
time: 237 us
  waiting for transfers between devices  162 us (68%)
  local copies, waits for them, and re-layouts  21.7 us (9%)
  between operations  13.8 us (6%)
  starting transfers between devices  10.6 us (4%)
  other arithmetic  10 us (4%)
  matrix products  9.17 us (4%)
  blocking collectives  9.16 us (4%)
    all_gather x1, waiting for transfers between devices, rows_first(): whole = lax.all_gather(both, axis, axis=0, tiled=True)  162 us
    all_to_all x1, blocking collectives, per_device(): lax.all_to_all(mixed_raw, 'tp', split_axis=0, concat_axis=1, tiled=True)  9.16 us
    ppermute x2, starting transfers between devices, passed_along(): return lax.ppermute(x, axis, pairs)  6.76 us
    reshape x4, local copies, waits for them, and re-layouts, rows_first(): b.reshape(-1, *t.shape[1:])  6.76 us
    unnamed x29, local copies, waits for them, and re-layouts  6.68 us
    dot_general x2, matrix products, per_device(): jnp.dot(mixed, out_whole, preferred_element_type=jnp.float32)  4.92 us
  transfers between devices with their start and end apart: 4, of which 1 were waited for; matrix products, arithmetic and copies ran while one was open for 7% of the time, Pallas kernels for 0%

commit v1 on v0

v1 whole, which is shorter than its diff:
```python
import functools

import jax
import jax.numpy as jnp
from jax import lax
from jax.experimental import pallas as pl
from jax.experimental.pallas import tpu as pltpu
from jax.sharding import PartitionSpec as P

EPS = 1e-06
MESH = pl.DeviceIdType.MESH
F32 = jnp.float32
BF16 = jnp.bfloat16
LANES = 128
HALO = 16
BLOCK = 16


def block_kernel(
    sizes,
    tokens,
    gate_in,
    gate_conv,
    value_in,
    out_weight,
    conv_taps,
    pre_gain,
    mix_gain,
    post_gain,
    result,
    gates0,
    gates1,
    outs0,
    outs1,
    tok,
    normed,
    branch,
    stream,
    mixed_all,
    mixed_norm,
    mixed_own,
    mixed_rows,
    squares,
    load_sem,
    inj_send,
    inj_recv,
    cross_send,
    cross_recv,
    ring_send,
    ring_recv_a,
    ring_recv,
    halo_send,
    halo_recv,
    x_send,
    x_recv,
    a_send,
    a_recv,
):
    chips, tp_size, depth, rows, width, chans = sizes
    channels = tp_size * chans
    total = rows + HALO
    share = rows // tp_size
    sp = lax.axis_index("sp")
    tp = lax.axis_index("tp")
    z = sp // 2
    core = lax.rem(sp, 2)
    sgn = 1 - 2 * core
    minus = (9 * chips) // 16
    reaches = (chips - 1 - minus, minus)

    def chip(k):
        return lax.rem(z + k + 2 * chips, chips)

    partner = {"sp": z * 2 + 1 - core}
    ahead = {"sp": chip(sgn) * 2 + core}
    behind = {"sp": chip(-sgn) * 2 + core}
    follower = {"sp": lax.rem(sp + 1, 2 * chips)}
    leader = {"sp": lax.rem(sp + 2 * chips - 1, 2 * chips)}
    across = {"sp": jnp.where(core == 1, lax.rem(sp + 1, 2 * chips), lax.rem(sp + 2 * chips - 1, 2 * chips))}
    right = {"tp": lax.rem(tp + 1, tp_size)}
    left = {"tp": lax.rem(tp + tp_size - 1, tp_size)}

    barrier = pltpu.get_barrier_semaphore()
    peers = [partner, ahead, behind, across]
    peers += [{"tp": lax.rem(tp + j, tp_size)} for j in range(1, tp_size)]
    for peer in peers:
        pl.semaphore_signal(barrier, inc=1, device_id=peer, device_id_type=MESH)

    mine = pl.ds(pl.multiple_of(sp * depth, depth), depth)
    gates = (gates0, gates1)
    outs = (outs0, outs1)
    loads = []
    for layer in range(2):
        for j, weight in enumerate((gate_in, gate_conv, value_in)):
            copy = pltpu.make_async_copy(
                weight.at[layer], gates[layer].at[mine, pl.ds(j * chans, chans)], load_sem.at[3 * layer + j]
            )
            copy.start()
            loads.append(copy)
    for layer in range(2):
        copy = pltpu.make_async_copy(out_weight.at[layer], outs[layer].at[mine], load_sem.at[6 + layer])
        copy.start()
        loads.append(copy)
    load_tok = pltpu.make_async_copy(tokens, tok.at[pl.ds(HALO, rows)], load_sem.at[8])
    load_tok.start()

    buffers = (gates0, outs0, gates1, outs1)

    def one(zz, cc):
        return pl.ds(pl.multiple_of((zz * 2 + cc) * depth, depth), depth)

    def both(zz):
        return pl.ds(pl.multiple_of(zz * 2 * depth, 2 * depth), 2 * depth)

    def to_partner(s):
        ref = buffers[s].at[mine]
        return pltpu.make_async_remote_copy(
            src_ref=ref, dst_ref=ref, send_sem=inj_send.at[s], recv_sem=inj_recv.at[s],
            device_id=partner, device_id_type=MESH,
        )

    def from_partner(s):
        ref = buffers[s].at[one(z, 1 - core)]
        return pltpu.make_async_remote_copy(
            src_ref=ref, dst_ref=ref, send_sem=inj_send.at[s], recv_sem=inj_recv.at[s],
            device_id=partner, device_id_type=MESH,
        )

    def along(s, block, sem):
        ref = buffers[s].at[block]
        return pltpu.make_async_remote_copy(
            src_ref=ref, dst_ref=ref, send_sem=ring_send.at[s], recv_sem=sem,
            device_id=ahead, device_id_type=MESH,
        )

    def over(s, block):
        ref = buffers[s].at[block]
        return pltpu.make_async_remote_copy(
            src_ref=ref, dst_ref=ref, send_sem=cross_send.at[s], recv_sem=cross_recv.at[s],
            device_id=partner, device_id_type=MESH,
        )

    def relay_a(k, sub, reach):
        block = one(chip(-sgn * k), sub)
        along(0, block, ring_recv_a.at[sub, k]).wait_recv()

        @pl.when(k < reach)
        def _():
            along(0, block, ring_recv_a.at[sub, k + 1]).start()

        over(0, block).start()

    def relay(s, k, reach):
        block = both(chip(-sgn * k))
        along(s, block, ring_recv.at[s - 1, k]).wait_recv()

        @pl.when(k < reach)
        def _():
            along(s, block, ring_recv.at[s - 1, k + 1]).start()

        over(s, block).start()

    def halo_copy():
        return pltpu.make_async_remote_copy(
            src_ref=tokens.at[pl.ds(rows - HALO, HALO)], dst_ref=tok.at[pl.ds(0, HALO)],
            send_sem=halo_send, recv_sem=halo_recv, device_id=follower, device_id_type=MESH,
        )

    for copy in loads[:3]:
        copy.wait()
    pl.semaphore_wait(barrier, len(peers))
    along(0, mine, ring_recv_a.at[core, 1]).start()
    to_partner(0).start()
    for copy in loads[3:]:
        copy.wait()
    for s in (1, 2, 3):
        to_partner(s).start()
    from_partner(0).wait_recv()
    along(0, one(z, 1 - core), ring_recv_a.at[1 - core, 1]).start()
    for s in (1, 2, 3):
        from_partner(s).wait_recv()
        along(s, both(z), ring_recv.at[s - 1, 1]).start()

    @pl.when(sp < 2 * chips - 1)
    def _():
        halo_copy().start()

    @pl.when(sp == 0)
    def _():
        tok[pl.ds(0, HALO), :] = jnp.zeros((HALO, width), BF16)

    load_tok.wait()
    blocks = total // BLOCK

    def norm_block(b):
        at = pl.ds(pl.multiple_of(lax.rem(b + 1, blocks) * BLOCK, BLOCK), BLOCK)
        x = tok[at, :].astype(F32)
        scale = lax.rsqrt(jnp.sum(x * x, axis=-1, keepdims=True) / width + EPS)
        normed[at, :] = (x * scale * pre_gain[pl.ds(0, 1), :]).astype(BF16)

    def norm_some(k, count):
        for j in range(count):
            b = (k - 1) * count + j

            @pl.when((b == blocks - 1) & (sp > 0))
            def _():
                halo_copy().wait_recv()

            @pl.when(b < blocks)
            def _():
                norm_block(b)

    for cc in range(2):

        @pl.when(core == cc)
        def _(reach=reaches[cc]):
            def step(k, carry):
                relay_a(k, core, reach)
                relay_a(k, 1 - core, reach)
                for s in (1, 2, 3):
                    relay(s, k, reach)
                norm_some(k, -(-blocks // reach))
                return carry

            lax.fori_loop(1, reach + 1, step, 0)

    def arrived(s):
        for cc in range(2):

            @pl.when(core == cc)
            def _():
                over(s, pl.ds(0, reaches[1 - cc] * 2 * depth)).wait_recv()

    def mixing(layer):
        product = jnp.dot(normed[...], gates[layer][...], preferred_element_type=F32)
        outer = product[:, :chans].astype(BF16).astype(F32)
        inner = product[:, chans : 2 * chans].astype(BF16).astype(F32)
        values = product[:, 2 * chans :].astype(BF16).astype(F32)
        gated = (inner * values).astype(BF16).astype(F32)
        here = pl.ds(pl.multiple_of(tp * chans, chans), chans)
        taps = conv_taps[:, layer, here]
        filtered = (
            taps[0:1, :] * pltpu.roll(gated, 2, axis=0)
            + taps[1:2, :] * pltpu.roll(gated, 1, axis=0)
            + taps[2:3, :] * gated
        )
        return (outer * filtered).astype(BF16)

    def mix_norm(raw, layer):
        x = raw.astype(F32)
        scale = lax.rsqrt(jnp.sum(x * x, axis=-1, keepdims=True) / channels + EPS)
        return (x * scale * mix_gain[pl.ds(layer, 1), :]).astype(BF16)

    def lanes(j):
        return pl.ds(pl.multiple_of(lax.rem(j + tp_size, tp_size) * chans, chans), chans)

    arrived(0)
    mixed_all[:, lanes(tp)] = mixing(0)
    half = (total // BLOCK + 1) // 2 * BLOCK
    parts = (pl.ds(0, half), pl.ds(half, total - half))

    def swap(i, part, owner, to):
        ref = mixed_all.at[parts[part], lanes(owner)]
        return pltpu.make_async_remote_copy(
            src_ref=ref, dst_ref=ref, send_sem=x_send.at[i], recv_sem=x_recv.at[i], device_id=to, device_id_type=MESH
        )

    swap(0, 0, tp, right).start()
    swap(2, 1, tp, left).start()
    swap(1, 1, tp, right).start()
    swap(3, 0, tp, left).start()
    swap(0, 0, tp - 1, right).wait_recv()
    swap(4, 0, tp - 1, right).start()
    swap(2, 1, tp + 1, left).wait_recv()
    swap(5, 1, tp + 1, left).start()

    arrived(1)
    swap(1, 1, tp - 1, right).wait_recv()
    swap(3, 0, tp + 1, left).wait_recv()
    swap(4, 0, tp + 2, right).wait_recv()
    swap(5, 1, tp + 2, left).wait_recv()
    mixed_norm[...] = mix_norm(mixed_all[...], 0)
    tile = 2 * LANES
    tiles = width // tile

    def fold(x):
        return x[:, :LANES] + x[:, LANES:]

    squares[...] = jnp.zeros_like(squares)

    def project(n, carry):
        cols = pl.ds(pl.multiple_of(n * tile, tile), tile)
        out = lax.dot_general(
            mixed_norm[...], outs0[cols, :], (((1,), (1,)), ((), ())), preferred_element_type=F32
        ).astype(BF16)
        branch[:, cols] = out
        wide = out.astype(F32)
        squares[...] += fold(wide * wide)
        return carry

    lax.fori_loop(0, tiles, project, 0)
    group = 3

    def next_stream(i, carry):
        for j in range(group):
            b = i * group + j

            @pl.when(b < blocks)
            def _():
                at = pl.ds(pl.multiple_of(b * BLOCK, BLOCK), BLOCK)
                ss = jnp.sum(squares[at, :], axis=-1, keepdims=True)
                scale = lax.rsqrt(ss / width + EPS)
                new = tok[at, :].astype(F32) + branch[at, :].astype(F32) * scale * post_gain[pl.ds(0, 1), :]
                stream[at, :] = new
                scale = lax.rsqrt(jnp.sum(new * new, axis=-1, keepdims=True) / width + EPS)
                normed[at, :] = (new * scale * pre_gain[pl.ds(1, 1), :]).astype(BF16)

        return carry

    lax.fori_loop(0, -(-blocks // group), next_stream, 0)
    arrived(2)

    mixed_own[...] = mixing(1)[HALO:, :]

    def spread(j):
        to = lax.rem(tp + j, tp_size)
        return pltpu.make_async_remote_copy(
            src_ref=mixed_own.at[pl.ds(pl.multiple_of(to * share, share), share)],
            dst_ref=mixed_rows.at[:, lanes(tp)],
            send_sem=a_send.at[j], recv_sem=a_recv.at[j], device_id={"tp": to}, device_id_type=MESH,
        )

    def gathered(j):
        ref = mixed_rows.at[:, lanes(tp - j)]
        return pltpu.make_async_remote_copy(
            src_ref=ref, dst_ref=ref, send_sem=a_send.at[j], recv_sem=a_recv.at[j],
            device_id={"tp": lax.rem(tp + j, tp_size)}, device_id_type=MESH,
        )

    order = [2, 1, 3] if tp_size == 4 else list(range(1, tp_size))
    for j in order:
        spread(j).start()
    own_rows = pl.ds(pl.multiple_of(tp * share, share), share)
    mixed_rows[:, lanes(tp)] = mixed_own[own_rows, :]
    arrived(3)
    for j in order:
        gathered(j).wait_recv()
    mixed = mix_norm(mixed_rows[...], 1)
    sums = jnp.zeros((share, LANES), F32)
    for n in range(tiles):
        cols = pl.ds(n * tile, tile)
        out = lax.dot_general(
            mixed, outs1[cols, :], (((1,), (1,)), ((), ())), preferred_element_type=F32
        ).astype(BF16)
        branch[pl.ds(0, share), cols] = out
        wide = out.astype(F32)
        sums = sums + fold(wide * wide)
    squares[pl.ds(0, share), :] = sums

    def finish(b, carry):
        at = pl.ds(pl.multiple_of(b * BLOCK, BLOCK), BLOCK)
        scale = lax.rsqrt(jnp.sum(squares[at, :], axis=-1, keepdims=True) / width + EPS)
        held = pl.ds(pl.multiple_of(HALO + tp * share + b * BLOCK, BLOCK), BLOCK)
        result[at, :] = (
            stream[held, :] + branch[at, :].astype(F32) * scale * post_gain[pl.ds(1, 1), :]
        ).astype(BF16)
        return carry

    lax.fori_loop(0, share // BLOCK, finish, 0)

    @pl.when(sp < 2 * chips - 1)
    def _():
        halo_copy().wait_send()

    for j in order:
        spread(j).wait_send()
    for i, part in ((0, 0), (1, 1), (2, 1), (3, 0), (4, 0), (5, 1)):
        swap(i, part, tp, right).wait_send()
    for s in range(4):
        to_partner(s).wait_send()
        for cc in range(2):
            reach = reaches[cc]

            @pl.when(core == cc)
            def _(s=s, reach=reach):
                sent = pl.ds(0, reach * 2 * depth)
                along(s, sent, ring_recv.at[0, 0]).wait_send()
                over(s, sent).wait_send()


def solution(mesh):
    chips = mesh.shape["sp"] // 2
    tp_size = mesh.shape["tp"]

    def per_device(tokens, gate_in, gate_conv, value_in, out_weight, conv_taps, pre_gain, mix_gain, post_gain):
        rows, width = tokens.shape
        depth, chans = gate_in.shape[1:]
        channels = tp_size * chans
        total = rows + HALO
        share = rows // tp_size
        sizes = (chips, tp_size, depth, rows, width, chans)
        anywhere = pl.BlockSpec(memory_space=pl.ANY)
        inside = pl.BlockSpec(memory_space=pltpu.VMEM)
        dma = pltpu.SemaphoreType.DMA
        return pl.pallas_call(
            functools.partial(block_kernel, sizes),
            out_shape=jax.ShapeDtypeStruct((share, width), BF16),
            in_specs=[anywhere] * 5 + [inside] * 4,
            out_specs=inside,
            scratch_shapes=[
                pltpu.VMEM((width, 3 * chans), BF16),
                pltpu.VMEM((width, 3 * chans), BF16),
                pltpu.VMEM((width, channels), BF16),
                pltpu.VMEM((width, channels), BF16),
                pltpu.VMEM((total, width), BF16),
                pltpu.VMEM((total, width), BF16),
                pltpu.VMEM((total, width), BF16),
                pltpu.VMEM((total, width), F32),
                pltpu.VMEM((total, channels), BF16),
                pltpu.VMEM((total, channels), BF16),
                pltpu.VMEM((rows, chans), BF16),
                pltpu.VMEM((share, channels), BF16),
                pltpu.VMEM((total, LANES), F32),
                dma((9,)),
                dma((4,)),
                dma((4,)),
                dma((4,)),
                dma((4,)),
                dma((4,)),
                dma((2, chips)),
                dma((3, chips)),
                dma,
                dma,
                dma((6,)),
                dma((6,)),
                dma((tp_size,)),
                dma((tp_size,)),
            ],
            compiler_params=pltpu.CompilerParams(
                collective_id=0, has_side_effects=True, vmem_limit_bytes=56 * 2**20
            ),
            name="blocks",
        )(
            tokens,
            gate_in,
            gate_conv,
            value_in,
            jnp.swapaxes(out_weight, 1, 2),
            jnp.swapaxes(conv_taps, 0, 1),
            pre_gain,
            mix_gain,
            post_gain,
        )

    return jax.shard_map(
        per_device,
        mesh=mesh,
        in_specs=(
            P(("grp", "sp"), None),
            P(None, "sp", "tp"),
            P(None, "sp", "tp"),
            P(None, "sp", "tp"),
            P(None, None, "sp"),
            P(),
            P(),
            P(),
            P(),
        ),
        out_specs=P(("grp", "sp", "tp"), None),
        check_vma=False,
    )
```

time: 237 us -> 119 us (0.50)
  waiting for transfers between devices: 162 us -> 0 us
  Pallas kernels: 0 us -> 117 us
  local copies, waits for them, and re-layouts: 21.7 us -> 1.88 us
  between operations: 13.8 us -> 0.01 us
  starting transfers between devices: 10.6 us -> 0 us
  other arithmetic: 10 us -> 0 us
  matrix products: 9.17 us -> 0 us
  blocking collectives: 9.16 us -> 0 us
    all_gather x1 -> x0, waiting for transfers between devices: 162 us -> none  [rows_first(): whole = lax.all_gather(both, axis, axis=0, tiled=True)]
    pallas_call x0 -> x1, Pallas kernels: none -> 117 us  [per_device(): pl.pallas_call(functools.partial(block_kernel, sizes), out_shape=jax.Shap...]
    reshape x7 -> x0, local copies, waits for them, and re-layouts: 9.2 us -> none  [the longest x4 6.76 us: rows_first(): b.reshape(-1, *t.shape[1:])]
    dot_general x8 -> x0, matrix products: 9.17 us -> none  [the longest x2 4.92 us: per_device(): jnp.dot(mixed, out_whole, preferred_element_type=jnp.float32)]
    all_to_all x1 -> x0, blocking collectives: 9.16 us -> none  [per_device(): lax.all_to_all(mixed_raw, 'tp', split_axis=0, concat_axis=1, tiled=True)]
    ppermute x2 -> x0, starting transfers between devices: 6.76 us -> none  [passed_along(): return lax.ppermute(x, axis, pairs)]
    convert_element_type x9 -> x0, other arithmetic: 5.2 us -> none  [the longest x8 2.95 us: stored(): return lax.optimization_barrier(values.astype(jnp.bfloat16))]
    unnamed x29 -> x1, local copies, waits for them, and re-layouts: 6.68 us -> 1.88 us
  transfers between devices with their start and end apart: 4 -> 0, of which waited for: 1 -> 0; matrix products, arithmetic and copies ran while one was open for 7% -> 0% of each run, Pallas kernels for 0% -> 0%
where the time goes in v1:
time: 119 us
  Pallas kernels  117 us (98%)
  local copies, waits for them, and re-layouts  1.88 us (2%)
    pallas_call x1, Pallas kernels, per_device(): pl.pallas_call(functools.partial(block_kernel, sizes), out_shape=jax.Shap...  117 us

profile of v1, /device:TPU:33, one launch (start us, length us, event | category | flops | bytes accessed | tf_op | source)
XLA Modules:
  0.0 119.1 jit_solution(8521482960785242980)
XLA Ops:
  0.0 117.2 %blocks.1 = bf16[128,2048]{1,0:T(8,128)(2,1)} custom-call(bf16[512,2048]{1,0:T(8,128)(2,1)} %tokens.1, bf16[2,32,128]{2,1,0:T(8,128)(2,1)} %gate_in.1, bf16[2,32,128]{2,1,0:T(8,128)(2,1)} %gate_conv.1, bf16[2,32,128]{2,1,0:T(8,128)(2,1)} %value_in.1, bf16[2,32,512]{2,1,0:T(8,128)(2,1)} %bitcast.2, f32[3,2,512]{2,1,0:T(2,128)} %bitcast.3, ...), custom_call_target="tpu_custom_call" | custom-call | tf_op jit(solution)/shard_map/blocks/pallas_call | solution.py:405
  117.2 1.9 %copy.11 = bf16[128,2048]{1,0:T(8,128)(2,1)} copy(bf16[128,2048]{1,0:T(8,128)(2,1)} %blocks.1) | data formatting | bytes 1048576

commit v2 on v1

--- a/solution.py
+++ b/solution.py
@@ -14,6 +14,7 @@
 LANES = 128
 HALO = 16
 BLOCK = 16
+LAG = 2
 
 
 def block_kernel(
@@ -30,8 +31,7 @@
     result,
     gates0,
     gates1,
-    outs0,
-    outs1,
+    outs,
     tok,
     normed,
     branch,
@@ -47,12 +47,13 @@
     cross_send,
     cross_recv,
     ring_send,
-    ring_recv_a,
     ring_recv,
     halo_send,
     halo_recv,
     x_send,
     x_recv,
+    spread_send,
+    spread_recv,
     a_send,
     a_recv,
 ):
@@ -88,7 +89,6 @@
 
     mine = pl.ds(pl.multiple_of(sp * depth, depth), depth)
     gates = (gates0, gates1)
-    outs = (outs0, outs1)
     loads = []
     for layer in range(2):
         for j, weight in enumerate((gate_in, gate_conv, value_in)):
@@ -98,13 +98,24 @@
             copy.start()
             loads.append(copy)
     for layer in range(2):
-        copy = pltpu.make_async_copy(out_weight.at[layer], outs[layer].at[mine], load_sem.at[6 + layer])
-        copy.start()
-        loads.append(copy)
-    load_tok = pltpu.make_async_copy(tokens, tok.at[pl.ds(HALO, rows)], load_sem.at[8])
+        for j in range(tp_size):
+            copy = pltpu.make_async_copy(
+                out_weight.at[layer, :, pl.ds(j * chans, chans)],
+                outs.at[mine, pl.ds((2 * j + layer) * chans, chans)],
+                load_sem.at[7 + layer * tp_size + j],
+            )
+            copy.start()
+            loads.append(copy)
+    load_tok = pltpu.make_async_copy(tokens, tok.at[pl.ds(HALO, rows)], load_sem.at[6])
     load_tok.start()
 
-    buffers = (gates0, outs0, gates1, outs1)
+    buffers = (gates0, gates1, outs)
+
+    def quarter(j):
+        return pl.ds(pl.multiple_of(lax.rem(j + tp_size, tp_size) * 2 * chans, 2 * chans), 2 * chans)
+
+    def part(s, block):
+        return outs.at[block, quarter(tp)] if s == 2 else buffers[s].at[block]
 
     def one(zz, cc):
         return pl.ds(pl.multiple_of((zz * 2 + cc) * depth, depth), depth)
@@ -126,39 +137,44 @@
             device_id=partner, device_id_type=MESH,
         )
 
-    def along(s, block, sem):
-        ref = buffers[s].at[block]
-        return pltpu.make_async_remote_copy(
-            src_ref=ref, dst_ref=ref, send_sem=ring_send.at[s], recv_sem=sem,
-            device_id=ahead, device_id_type=MESH,
-        )
-
-    def over(s, block):
-        ref = buffers[s].at[block]
-        return pltpu.make_async_remote_copy(
-            src_ref=ref, dst_ref=ref, send_sem=cross_send.at[s], recv_sem=cross_recv.at[s],
+    def along(s, block, sem, to):
+        ref = part(s, block)
+        return pltpu.make_async_remote_copy(
+            src_ref=ref, dst_ref=ref, send_sem=ring_send.at[s], recv_sem=sem, device_id=to, device_id_type=MESH
+        )
+
+    def cross(i, ref):
+        return pltpu.make_async_remote_copy(
+            src_ref=ref, dst_ref=ref, send_sem=cross_send.at[i], recv_sem=cross_recv.at[i],
             device_id=partner, device_id_type=MESH,
         )
 
-    def relay_a(k, sub, reach):
-        block = one(chip(-sgn * k), sub)
-        along(0, block, ring_recv_a.at[sub, k]).wait_recv()
-
+    def launch(s, block, k, sub, reach):
         @pl.when(k < reach)
         def _():
-            along(0, block, ring_recv_a.at[sub, k + 1]).start()
-
-        over(0, block).start()
-
-    def relay(s, k, reach):
-        block = both(chip(-sgn * k))
-        along(s, block, ring_recv.at[s - 1, k]).wait_recv()
-
-        @pl.when(k < reach)
-        def _():
-            along(s, block, ring_recv.at[s - 1, k + 1]).start()
-
-        over(s, block).start()
+            along(s, block, ring_recv.at[s, sub, k + 1], ahead).start()
+
+    def relay(s, k, sub, reach):
+        block = one(chip(-sgn * k), sub)
+        along(s, block, ring_recv.at[s, sub, k], ahead).wait_recv()
+        launch(s, block, k, sub, reach)
+        cross(s, part(s, block)).start()
+
+    def quarter_to(k, j):
+        ref = outs.at[both(chip(-sgn * k)), quarter(tp)]
+        return pltpu.make_async_remote_copy(
+            src_ref=ref, dst_ref=ref, send_sem=spread_send, recv_sem=spread_recv.at[j - 1, k],
+            device_id={"tp": lax.rem(tp + j, tp_size)}, device_id_type=MESH,
+        )
+
+    def quarters_in(k):
+        for j in range(1, tp_size):
+            ref = outs.at[both(chip(-sgn * k)), quarter(tp - j)]
+            pltpu.make_async_remote_copy(
+                src_ref=ref, dst_ref=ref, send_sem=spread_send, recv_sem=spread_recv.at[j - 1, k],
+                device_id={"tp": lax.rem(tp + j, tp_size)}, device_id_type=MESH,
+            ).wait_recv()
+            cross(3, ref).start()
 
     def halo_copy():
         return pltpu.make_async_remote_copy(
@@ -169,17 +185,17 @@
     for copy in loads[:3]:
         copy.wait()
     pl.semaphore_wait(barrier, len(peers))
-    along(0, mine, ring_recv_a.at[core, 1]).start()
+    reach_here = jnp.where(core == 1, reaches[1], reaches[0])
+    launch(0, mine, 0, core, reach_here)
     to_partner(0).start()
     for copy in loads[3:]:
         copy.wait()
-    for s in (1, 2, 3):
+    for s in (2, 1):
+        launch(s, mine, 0, core, reach_here)
         to_partner(s).start()
-    from_partner(0).wait_recv()
-    along(0, one(z, 1 - core), ring_recv_a.at[1 - core, 1]).start()
-    for s in (1, 2, 3):
+    for s in (0, 2, 1):
         from_partner(s).wait_recv()
-        along(s, both(z), ring_recv.at[s - 1, 1]).start()
+        launch(s, one(z, 1 - core), 0, 1 - core, reach_here)
 
     @pl.when(sp < 2 * chips - 1)
     def _():
@@ -215,21 +231,34 @@
         @pl.when(core == cc)
         def _(reach=reaches[cc]):
             def step(k, carry):
-                relay_a(k, core, reach)
-                relay_a(k, 1 - core, reach)
-                for s in (1, 2, 3):
-                    relay(s, k, reach)
+                for s in (0, 2, 1):
+                    relay(s, k, core, reach)
+                    relay(s, k, 1 - core, reach)
+                    if s == 2:
+                        for j in range(1, tp_size):
+                            quarter_to(k, j).start()
                 norm_some(k, -(-blocks // reach))
+
+                @pl.when(k > LAG)
+                def _():
+                    quarters_in(k - LAG)
+
                 return carry
 
             lax.fori_loop(1, reach + 1, step, 0)
 
-    def arrived(s):
+    def covering(i, reach):
+        held = pl.ds(0, reach * 2 * depth)
+        if i < 2:
+            return buffers[i].at[held]
+        return outs.at[held, pl.ds(0, 2 * chans * (1 if i == 2 else tp_size - 1))]
+
+    def arrived(i):
         for cc in range(2):
 
             @pl.when(core == cc)
             def _():
-                over(s, pl.ds(0, reaches[1 - cc] * 2 * depth)).wait_recv()
+                cross(i, covering(i, reaches[1 - cc])).wait_recv()
 
     def mixing(layer):
         product = jnp.dot(normed[...], gates[layer][...], preferred_element_type=F32)
@@ -274,7 +303,10 @@
     swap(2, 1, tp + 1, left).wait_recv()
     swap(5, 1, tp + 1, left).start()
 
-    arrived(1)
+    for lag in reversed(range(LAG)):
+        quarters_in(reach_here - lag)
+    arrived(2)
+    arrived(3)
     swap(1, 1, tp - 1, right).wait_recv()
     swap(3, 0, tp + 1, left).wait_recv()
     swap(4, 0, tp + 2, right).wait_recv()
@@ -283,6 +315,11 @@
     tile = 2 * LANES
     tiles = width // tile
 
+    def weights(cols, layer):
+        return jnp.concatenate(
+            [outs[cols, pl.ds((2 * j + layer) * chans, chans)] for j in range(tp_size)], axis=1
+        )
+
     def fold(x):
         return x[:, :LANES] + x[:, LANES:]
 
@@ -291,7 +328,7 @@
     def project(n, carry):
         cols = pl.ds(pl.multiple_of(n * tile, tile), tile)
         out = lax.dot_general(
-            mixed_norm[...], outs0[cols, :], (((1,), (1,)), ((), ())), preferred_element_type=F32
+            mixed_norm[...], weights(cols, 0), (((1,), (1,)), ((), ())), preferred_element_type=F32
         ).astype(BF16)
         branch[:, cols] = out
         wide = out.astype(F32)
@@ -318,7 +355,7 @@
         return carry
 
     lax.fori_loop(0, -(-blocks // group), next_stream, 0)
-    arrived(2)
+    arrived(1)
 
     mixed_own[...] = mixing(1)[HALO:, :]
 
@@ -342,7 +379,6 @@
         spread(j).start()
     own_rows = pl.ds(pl.multiple_of(tp * share, share), share)
     mixed_rows[:, lanes(tp)] = mixed_own[own_rows, :]
-    arrived(3)
     for j in order:
         gathered(j).wait_recv()
     mixed = mix_norm(mixed_rows[...], 1)
@@ -350,7 +386,7 @@
     for n in range(tiles):
         cols = pl.ds(n * tile, tile)
         out = lax.dot_general(
-            mixed, outs1[cols, :], (((1,), (1,)), ((), ())), preferred_element_type=F32
+            mixed, weights(cols, 1), (((1,), (1,)), ((), ())), preferred_element_type=F32
         ).astype(BF16)
         branch[pl.ds(0, share), cols] = out
         wide = out.astype(F32)
@@ -376,16 +412,24 @@
         spread(j).wait_send()
     for i, part in ((0, 0), (1, 1), (2, 1), (3, 0), (4, 0), (5, 1)):
         swap(i, part, tp, right).wait_send()
-    for s in range(4):
+    for s in range(3):
         to_partner(s).wait_send()
-        for cc in range(2):
-            reach = reaches[cc]
-
-            @pl.when(core == cc)
-            def _(s=s, reach=reach):
-                sent = pl.ds(0, reach * 2 * depth)
-                along(s, sent, ring_recv.at[0, 0]).wait_send()
-                over(s, sent).wait_send()
+    for cc in range(2):
+
+        @pl.when(core == cc)
+        def _(reach=reaches[cc]):
+            for i in range(4):
+                cross(i, covering(i, reach)).wait_send()
+            for i in range(3):
+                along_all = pltpu.make_async_remote_copy(
+                    src_ref=covering(i, reach), dst_ref=covering(i, reach), send_sem=ring_send.at[i],
+                    recv_sem=ring_recv.at[0, 0, 0], device_id=ahead, device_id_type=MESH,
+                )
+                along_all.wait_send()
+            pltpu.make_async_remote_copy(
+                src_ref=covering(3, reach), dst_ref=covering(3, reach), send_sem=spread_send,
+                recv_sem=ring_recv.at[0, 0, 0], device_id=right, device_id_type=MESH,
+            ).wait_send()
 
 
 def solution(mesh):
@@ -410,8 +454,7 @@
             scratch_shapes=[
                 pltpu.VMEM((width, 3 * chans), BF16),
                 pltpu.VMEM((width, 3 * chans), BF16),
-                pltpu.VMEM((width, channels), BF16),
-                pltpu.VMEM((width, channels), BF16),
+                pltpu.VMEM((width, 2 * channels), BF16),
                 pltpu.VMEM((total, width), BF16),
                 pltpu.VMEM((total, width), BF16),
                 pltpu.VMEM((total, width), BF16),
@@ -421,18 +464,19 @@
                 pltpu.VMEM((rows, chans), BF16),
                 pltpu.VMEM((share, channels), BF16),
                 pltpu.VMEM((total, LANES), F32),
-                dma((9,)),
+                dma((7 + 2 * tp_size,)),
                 dma((4,)),
                 dma((4,)),
                 dma((4,)),
                 dma((4,)),
                 dma((4,)),
-                dma((2, chips)),
-                dma((3, chips)),
+                dma((3, 2, chips)),
                 dma,
                 dma,
                 dma((6,)),
                 dma((6,)),
+                dma,
+                dma((tp_size - 1, chips)),
                 dma((tp_size,)),
                 dma((tp_size,)),
             ],

time: 119 us -> 112 us (0.941); the launches traced: 119 us -> 110 us
  Pallas kernels: 117 us -> 108 us
    pallas_call x1, Pallas kernels: 117 us -> 108 us  [per_device(): pl.pallas_call(functools.partial(block_kernel, sizes), out_shape=jax.Shap...]
where the time goes in v2:
time: 112 us; the launch traced here: 110 us
  Pallas kernels  108 us (96%)
  local copies, waits for them, and re-layouts  1.88 us (2%)
    pallas_call x1, Pallas kernels, per_device(): pl.pallas_call(functools.partial(block_kernel, sizes), out_shape=jax.Shap...  108 us

profile of v2, /device:TPU:33, one launch (start us, length us, event | category | flops | bytes accessed | tf_op | source)
XLA Modules:
  0.0 110.2 jit_solution(9467705369046779282)
XLA Ops:
  0.0 108.4 %blocks.1 = bf16[128,2048]{1,0:T(8,128)(2,1)} custom-call(bf16[512,2048]{1,0:T(8,128)(2,1)} %tokens.1, bf16[2,32,128]{2,1,0:T(8,128)(2,1)} %gate_in.1, bf16[2,32,128]{2,1,0:T(8,128)(2,1)} %gate_conv.1, bf16[2,32,128]{2,1,0:T(8,128)(2,1)} %value_in.1, bf16[2,32,512]{2,1,0:T(8,128)(2,1)} %bitcast.2, f32[3,2,512]{2,1,0:T(2,128)} %bitcast.3, ...), custom_call_target="tpu_custom_call" | custom-call | tf_op jit(solution)/shard_map/blocks/pallas_call | solution.py:449
  108.4 1.9 %copy.11 = bf16[128,2048]{1,0:T(8,128)(2,1)} copy(bf16[128,2048]{1,0:T(8,128)(2,1)} %blocks.1) | data formatting | bytes 1048576

commit v3 on v2

--- a/solution.py
+++ b/solution.py
@@ -336,25 +336,38 @@
         return carry
 
     lax.fori_loop(0, tiles, project, 0)
-    group = 3
+    group = max(g for g in (4, 3, 2, 1) if blocks % g == 0) * BLOCK
+    strips = width // LANES
+
+    def row_scale(sums):
+        return jnp.broadcast_to(lax.rsqrt(jnp.sum(sums, axis=-1, keepdims=True) / width + EPS), sums.shape)
+
+    squares[...] = row_scale(squares[...])
 
     def next_stream(i, carry):
-        for j in range(group):
-            b = i * group + j
-
-            @pl.when(b < blocks)
-            def _():
-                at = pl.ds(pl.multiple_of(b * BLOCK, BLOCK), BLOCK)
-                ss = jnp.sum(squares[at, :], axis=-1, keepdims=True)
-                scale = lax.rsqrt(ss / width + EPS)
-                new = tok[at, :].astype(F32) + branch[at, :].astype(F32) * scale * post_gain[pl.ds(0, 1), :]
-                stream[at, :] = new
-                scale = lax.rsqrt(jnp.sum(new * new, axis=-1, keepdims=True) / width + EPS)
-                normed[at, :] = (new * scale * pre_gain[pl.ds(1, 1), :]).astype(BF16)
-
+        at = pl.ds(pl.multiple_of(i * group, BLOCK), group)
+        scale = squares[at, :]
+        sums = jnp.zeros((group, LANES), F32)
+        for n in range(strips):
+            cols = pl.ds(n * LANES, LANES)
+            new = tok[at, cols].astype(F32) + branch[at, cols].astype(F32) * scale * post_gain[pl.ds(0, 1), cols]
+            stream[at, cols] = new
+            sums = sums + new * new
+        squares[at, :] = sums
         return carry
 
-    lax.fori_loop(0, -(-blocks // group), next_stream, 0)
+    lax.fori_loop(0, total // group, next_stream, 0)
+    squares[...] = row_scale(squares[...])
+
+    def next_normed(i, carry):
+        at = pl.ds(pl.multiple_of(i * group, BLOCK), group)
+        scale = squares[at, :]
+        for n in range(strips):
+            cols = pl.ds(n * LANES, LANES)
+            normed[at, cols] = (stream[at, cols] * scale * pre_gain[pl.ds(1, 1), cols]).astype(BF16)
+        return carry
+
+    lax.fori_loop(0, total // group, next_normed, 0)
     arrived(1)
 
     mixed_own[...] = mixing(1)[HALO:, :]
@@ -391,18 +404,12 @@
         branch[pl.ds(0, share), cols] = out
         wide = out.astype(F32)
         sums = sums + fold(wide * wide)
-    squares[pl.ds(0, share), :] = sums
-
-    def finish(b, carry):
-        at = pl.ds(pl.multiple_of(b * BLOCK, BLOCK), BLOCK)
-        scale = lax.rsqrt(jnp.sum(squares[at, :], axis=-1, keepdims=True) / width + EPS)
-        held = pl.ds(pl.multiple_of(HALO + tp * share + b * BLOCK, BLOCK), BLOCK)
-        result[at, :] = (
-            stream[held, :] + branch[at, :].astype(F32) * scale * post_gain[pl.ds(1, 1), :]
-        ).astype(BF16)
-        return carry
-
-    lax.fori_loop(0, share // BLOCK, finish, 0)
+    scale = row_scale(sums)
+    held = pl.ds(pl.multiple_of(HALO + tp * share, BLOCK), share)
+    for n in range(strips):
+        cols = pl.ds(n * LANES, LANES)
+        new = stream[held, cols] + branch[pl.ds(0, share), cols].astype(F32) * scale * post_gain[pl.ds(1, 1), cols]
+        result[:, cols] = new.astype(BF16)
 
     @pl.when(sp < 2 * chips - 1)
     def _():

time: 112 us -> 106 us (0.946)
  Pallas kernels: 108 us -> 103 us
    pallas_call x1, Pallas kernels: 108 us -> 103 us  [per_device(): pl.pallas_call(functools.partial(block_kernel, sizes), out_shape=jax.Shap...]
where the time goes in v3:
time: 106 us; the launch traced here: 105 us
  Pallas kernels  103 us (97%)
  local copies, waits for them, and re-layouts  1.88 us (2%)
    pallas_call x1, Pallas kernels, per_device(): pl.pallas_call(functools.partial(block_kernel, sizes), out_shape=jax.Shap...  103 us

profile of v3, /device:TPU:33, one launch (start us, length us, event | category | flops | bytes accessed | tf_op | source)
XLA Modules:
  0.0 104.5 jit_solution(6117393319084120238)
XLA Ops:
  0.0 102.6 %blocks.1 = bf16[128,2048]{1,0:T(8,128)(2,1)} custom-call(bf16[512,2048]{1,0:T(8,128)(2,1)} %tokens.1, bf16[2,32,128]{2,1,0:T(8,128)(2,1)} %gate_in.1, bf16[2,32,128]{2,1,0:T(8,128)(2,1)} %gate_conv.1, bf16[2,32,128]{2,1,0:T(8,128)(2,1)} %value_in.1, bf16[2,32,512]{2,1,0:T(8,128)(2,1)} %bitcast.2, f32[3,2,512]{2,1,0:T(2,128)} %bitcast.3, ...), custom_call_target="tpu_custom_call" | custom-call | tf_op jit(solution)/shard_map/blocks/pallas_call | solution.py:456
  102.6 1.9 %copy.11 = bf16[128,2048]{1,0:T(8,128)(2,1)} copy(bf16[128,2048]{1,0:T(8,128)(2,1)} %blocks.1) | data formatting | bytes 1048576

commit v4 on v3

--- a/solution.py
+++ b/solution.py
@@ -285,32 +285,24 @@
 
     arrived(0)
     mixed_all[:, lanes(tp)] = mixing(0)
-    half = (total // BLOCK + 1) // 2 * BLOCK
-    parts = (pl.ds(0, half), pl.ds(half, total - half))
-
-    def swap(i, part, owner, to):
-        ref = mixed_all.at[parts[part], lanes(owner)]
-        return pltpu.make_async_remote_copy(
-            src_ref=ref, dst_ref=ref, send_sem=x_send.at[i], recv_sem=x_recv.at[i], device_id=to, device_id_type=MESH
-        )
-
-    swap(0, 0, tp, right).start()
-    swap(2, 1, tp, left).start()
-    swap(1, 1, tp, right).start()
-    swap(3, 0, tp, left).start()
-    swap(0, 0, tp - 1, right).wait_recv()
-    swap(4, 0, tp - 1, right).start()
-    swap(2, 1, tp + 1, left).wait_recv()
-    swap(5, 1, tp + 1, left).start()
+
+    def swap(j, owner):
+        ref = mixed_all.at[:, lanes(owner)]
+        return pltpu.make_async_remote_copy(
+            src_ref=ref, dst_ref=ref, send_sem=x_send.at[j], recv_sem=x_recv.at[j],
+            device_id={"tp": lax.rem(tp + j, tp_size)}, device_id_type=MESH,
+        )
+
+    order = [2, 1, 3] if tp_size == 4 else list(range(1, tp_size))
+    for j in order:
+        swap(j, tp).start()
 
     for lag in reversed(range(LAG)):
         quarters_in(reach_here - lag)
     arrived(2)
     arrived(3)
-    swap(1, 1, tp - 1, right).wait_recv()
-    swap(3, 0, tp + 1, left).wait_recv()
-    swap(4, 0, tp + 2, right).wait_recv()
-    swap(5, 1, tp + 2, left).wait_recv()
+    for j in order:
+        swap(j, tp - j).wait_recv()
     mixed_norm[...] = mix_norm(mixed_all[...], 0)
     tile = 2 * LANES
     tiles = width // tile
@@ -417,8 +409,8 @@
 
     for j in order:
         spread(j).wait_send()
-    for i, part in ((0, 0), (1, 1), (2, 1), (3, 0), (4, 0), (5, 1)):
-        swap(i, part, tp, right).wait_send()
+    for j in order:
+        swap(j, tp).wait_send()
     for s in range(3):
         to_partner(s).wait_send()
     for cc in range(2):

time: 106 us -> 106 us (level); the launches traced: 105 us -> 106 us
    pallas_call x1, Pallas kernels: 103 us -> 104 us  [per_device(): pl.pallas_call(functools.partial(block_kernel, sizes), out_shape=jax.Shap...]
where the time goes in v4:
time: 106 us
  Pallas kernels  104 us (98%)
  local copies, waits for them, and re-layouts  1.88 us (2%)
    pallas_call x1, Pallas kernels, per_device(): pl.pallas_call(functools.partial(block_kernel, sizes), out_shape=jax.Shap...  104 us

profile of v4, /device:TPU:33, one launch (start us, length us, event | category | flops | bytes accessed | tf_op | source)
XLA Modules:
  0.0 105.7 jit_solution(8069763044660630564)
XLA Ops:
  0.0 103.8 %blocks.1 = bf16[128,2048]{1,0:T(8,128)(2,1)} custom-call(bf16[512,2048]{1,0:T(8,128)(2,1)} %tokens.1, bf16[2,32,128]{2,1,0:T(8,128)(2,1)} %gate_in.1, bf16[2,32,128]{2,1,0:T(8,128)(2,1)} %gate_conv.1, bf16[2,32,128]{2,1,0:T(8,128)(2,1)} %value_in.1, bf16[2,32,512]{2,1,0:T(8,128)(2,1)} %bitcast.2, f32[3,2,512]{2,1,0:T(2,128)} %bitcast.3, ...), custom_call_target="tpu_custom_call" | custom-call | tf_op jit(solution)/shard_map/blocks/pallas_call | solution.py:448
  103.8 1.9 %copy.11 = bf16[128,2048]{1,0:T(8,128)(2,1)} copy(bf16[128,2048]{1,0:T(8,128)(2,1)} %blocks.1) | data formatting | bytes 1048576
